TPU v7x, 32 devices: a whole 2x2x4 slice. The times are simulated.
32 devices in a mesh: fs: 16 (over z, y, x), tp: 2 (over core).
Axes of the slice: x: 2, y: 2, z: 4, core: 2. Of those that a mesh axis runs over, the one named last changes fastest.
Arguments:
- inputs: bfloat16 [8192, 2048], P('fs', 'tp'), may hold values from -6 to 6
- value_cotangent: bfloat16 [8192, 2048], P('fs', 'tp'), may hold values from -6 to 6
- first_map: bfloat16 [8192, 2048], P('fs', 'tp'), may hold values from -6 to 6
- second_map: bfloat16 [8192, 2048], P('fs', 'tp'), may hold values from -6 to 6
- lambdas: float32 [16], P('tp'), may hold values from 0.3 to 0.8
- head_gain: float32 [128], replicated, may hold values from 0.1 to 1.9
- output_cotangent: bfloat16 [8192, 2048], P('fs', 'tp'), may hold values from -6 to 6
- value_factor: bfloat16 [2048, 256], replicated, may hold values from -0.125 to 0.125
- output_factor: bfloat16 [2048, 256], replicated, may hold values from -0.125 to 0.125
- value_weight: float32 [2048, 2048], P('fs', 'tp'), may hold values from -0.125 to 0.125
- output_weight: float32 [2048, 2048], P('tp', 'fs'), may hold values from -0.125 to 0.125
- value_moment: float32 [256, 2048], P('fs', 'tp'), may hold values from -6 to 6
- value_second: float32 [256, 2048], P('fs', 'tp'), may hold values from 0.25 to 4
- output_moment: float32 [256, 2048], P('fs', 'tp'), may hold values from -6 to 6
- output_second: float32 [256, 2048], P('fs', 'tp'), may hold values from 0.25 to 4
Outputs:
- value_master: float32 [2048, 2048], P('fs', 'tp')
- output_master: float32 [2048, 2048], P('tp', 'fs')
- value_moment_new: float32 [256, 2048], P('fs', 'tp')
- value_second_new: float32 [256, 2048], P('fs', 'tp')
- output_moment_new: float32 [256, 2048], P('fs', 'tp')
- output_second_new: float32 [256, 2048], P('fs', 'tp')
- value_copy: bfloat16 [2048, 2048], P(None, 'tp')
- output_copy: bfloat16 [2048, 2048], P('tp')
All inputs are finite; a program needn't handle non-finite values.
Results may differ from a plain program's by a relative error of at most 0.0027.
Values may be sent and summed in bfloat16 or wider, within the bound.
A program may use at most 64 MiB of HBM per device.

v0:
```python
import math
import jax
import jax.numpy as jnp
from jax import lax
from jax.sharding import PartitionSpec as P


def contract_rows(left, right, precise):
    if precise:
        return lax.dot_general(
            left,
            right,
            (((0,), (0,)), ((), ())),
            precision=lax.Precision.HIGHEST,
            preferred_element_type=jnp.float32,
        )
    return lax.dot_general(
        left, right, (((0,), (0,)), ((), ())), preferred_element_type=jnp.float32
    )


def local(
    inputs,
    value_cotangent,
    first_map,
    second_map,
    lambdas,
    head_gain,
    output_cotangent,
    value_factor,
    output_factor,
    value_weight,
    output_weight,
    value_moment,
    value_second,
    output_moment,
    output_second,
):
    tok_rows = inputs.shape[0]
    local_heads = lambdas.shape[0]
    head_width = head_gain.shape[0]
    head_cols = local_heads * head_width
    first = first_map.astype(jnp.float32).reshape(tok_rows, local_heads, head_width)
    second = second_map.astype(jnp.float32).reshape(tok_rows, local_heads, head_width)
    difference = first - lambdas[None, :, None] * second
    normed = (
        difference
        * lax.rsqrt(jnp.mean(difference * difference, axis=-1, keepdims=True) + 1e-06)
        * head_gain
    )
    heads_out = normed.reshape(tok_rows, head_cols).astype(jnp.bfloat16)
    full_inputs, full_cotangent = (
        lax.all_gather(inputs, "tp", axis=1, tiled=True),
        lax.all_gather(output_cotangent, "tp", axis=1, tiled=True),
    )
    token_scale = 1.0 / math.sqrt(tok_rows * lax.axis_size("fs"))
    fs_index = lax.axis_index("fs")
    width_rows = value_weight.shape[0]
    value_rows = lax.dynamic_slice_in_dim(
        value_factor, fs_index * width_rows, width_rows, 0
    ).astype(jnp.float32)
    output_rows = lax.dynamic_slice_in_dim(
        output_factor, fs_index * width_rows, width_rows, 0
    ).astype(jnp.float32)
    grad_value = contract_rows(full_inputs, value_cotangent, False) * token_scale
    grad_output = contract_rows(full_cotangent, heads_out, False) * token_scale
    partial_value = jnp.concatenate(
        [
            contract_rows(value_factor.astype(jnp.float32), grad_value, True),
            contract_rows(output_factor.astype(jnp.float32), grad_output, True),
        ],
        axis=1,
    )
    own_rows = lax.psum_scatter(partial_value, "fs", scatter_dimension=0, tiled=True)
    moments = jnp.concatenate([value_moment, output_moment], axis=1)
    seconds = jnp.concatenate([value_second, output_second], axis=1)
    moment_new = 0.8 * moments + 0.2 * own_rows
    second_new = 0.95 * seconds + 0.05 * own_rows * own_rows
    direction = moment_new / (jnp.sqrt(second_new) + 1e-08)
    full_direction = lax.all_gather(direction, "fs", axis=0, tiled=True)
    step_value = jnp.dot(
        value_rows,
        full_direction[:, :head_cols],
        precision=lax.Precision.HIGHEST,
        preferred_element_type=jnp.float32,
    )
    step_output = jnp.dot(
        output_rows,
        full_direction[:, head_cols:],
        precision=lax.Precision.HIGHEST,
        preferred_element_type=jnp.float32,
    )
    value_master = value_weight - 0.05 * step_value
    output_master = output_weight - 0.05 * step_output.T
    value_copy, output_copy = (
        lax.all_gather(value_master.astype(jnp.bfloat16), "fs", axis=0, tiled=True),
        lax.all_gather(output_master.astype(jnp.bfloat16), "fs", axis=1, tiled=True),
    )
    return (
        value_master,
        output_master,
        moment_new[:, :head_cols],
        second_new[:, :head_cols],
        moment_new[:, head_cols:],
        second_new[:, head_cols:],
        value_copy,
        output_copy,
    )


def solution(mesh):
    in_specs = (
        P("fs", "tp"),
        P("fs", "tp"),
        P("fs", "tp"),
        P("fs", "tp"),
        P("tp"),
        P(),
        P("fs", "tp"),
        P(),
        P(),
        P("fs", "tp"),
        P("tp", "fs"),
        P("fs", "tp"),
        P("fs", "tp"),
        P("fs", "tp"),
        P("fs", "tp"),
    )
    out_specs = (
        P("fs", "tp"),
        P("tp", "fs"),
        P("fs", "tp"),
        P("fs", "tp"),
        P("fs", "tp"),
        P("fs", "tp"),
        P(None, "tp"),
        P("tp", None),
    )
    return jax.shard_map(local, mesh=mesh, in_specs=in_specs, out_specs=out_specs, check_vma=False)
```

profile of v0, /device:TPU:0, one launch (start us, length us, event | category | flops | bytes accessed | tf_op | source)
XLA Modules:
  0.0 374.0 jit_solution(844891537116236253)
XLA Ops:
  7.2 0.7 all-gather.8.cloned.1.call-update
  8.0 0.7 all-gather.6.cloned.1.call-update
  9.5 0.7 copy-done.2
  11.4 0.6 multiply_reduce_fusion
  12.4 10.5 %all-gather.8.cloned.1.call-done = bf16[512,2048]{1,0:T(8,128)(2,1)} async-done(((bf16[512,1024]{1,0:T(8,128)(2,1)}), bf16[512,2048]{1,0:T(8,128)(2,1)}) %all-gather.8.cloned.1.call-update) | async-done | bytes 2097168 | tf_op jit(solution)/shard_map/all_gather | solution.py:54
  22.9 0.6 mul.105
  23.5 1.0 copy-done.5
  24.5 2.8 fusion.18
  27.3 4.0 %fusion.13 = f32[256,1024]{0,1:T(8,128)S(1)} fusion(bf16[2048,256]{1,0:T(8,128)(2,1)S(1)} %copy-done.8, f32[1024,2048]{1,0:T(8,128)S(1)} %fusion.18), kind=kOutput, calls=%fused_computation.18 | convolution fusion | flops 6444548096 | bytes 10485760 | tf_op jit(solution)/shard_map/dot_general | solution.py:10
  31.4 4.8 %all-gather.6.cloned.1.call-done = bf16[512,2048]{1,0:T(8,128)(2,1)} async-done(((bf16[512,1024]{1,0:T(8,128)(2,1)}), bf16[512,2048]{1,0:T(8,128)(2,1)}) %all-gather.6.cloned.1.call-update) | async-done | bytes 2097168 | tf_op jit(solution)/shard_map/all_gather | solution.py:53
  36.2 4.0 %fusion.38 = f32[2048,1024]{1,0:T(8,128)S(1)} fusion(bf16[512,2048]{1,0:T(8,128)(2,1)} %all-gather.6.cloned.1.call-done, bf16[512,1024]{1,0:T(8,128)(2,1)S(1)} %copy-done), kind=kOutput, calls=%fused_computation.47 | convolution fusion | flops 2147483648 | bytes 11534336 | tf_op jit(solution)/shard_map/dot_general | solution.py:17
  40.2 6.9 %fusion.10 = f32[256,1024]{0,1:T(8,128)S(1)} fusion(bf16[2048,256]{1,0:T(8,128)(2,1)S(1)} %copy-done.7, f32[2048,1024]{1,0:T(8,128)S(1)} %fusion.38), kind=kOutput, calls=%fused_computation.17 | convolution fusion | flops 6444548096 | bytes 10485760 | tf_op jit(solution)/shard_map/dot_general | solution.py:10
  47.3 1.8 copy.49
  49.3 82.7 %reduce-scatter.4.cloned.1.call-done = f32[16,2048]{1,0:T(8,128)} async-done(((f32[256,2048]{1,0:T(8,128)}), f32[16,2048]{1,0:T(8,128)}) %reduce-scatter.4.cloned.1.call-update) | async-done | bytes 131088 | tf_op jit(solution)/shard_map/reduce_scatter | solution.py:74
  132.0 1.6 add_divide_fusion
  133.7 58.5 %all-gather.10.cloned.1.call-done = f32[256,2048]{1,0:T(8,128)} async-done(((f32[16,2048]{1,0:T(8,128)}), f32[256,2048]{1,0:T(8,128)}) %all-gather.10.cloned.1.call-update) | async-done | bytes 2097168 | tf_op jit(solution)/shard_map/all_gather | solution.py:80
  192.2 2.8 fusion.36
  195.1 2.7 fusion.37
  197.8 0.7 fusion.35
  198.5 0.7 fusion.34
  199.1 70.7 %all-gather.12.cloned.1.call-done = bf16[2048,1024]{1,0:T(8,128)(2,1)} async-done(((bf16[128,1024]{1,0:T(8,128)(2,1)}), bf16[2048,1024]{1,0:T(8,128)(2,1)}) %all-gather.12.cloned.1.call-update) | async-done | bytes 4194320 | tf_op jit(solution)/shard_map/all_gather | solution.py:96
  269.8 90.5 %all-gather.14.cloned.1.call-done = bf16[1024,2048]{1,0:T(8,128)(2,1)} async-done(((bf16[1024,128]{1,0:T(8,128)(2,1)}), bf16[1024,2048]{1,0:T(8,128)(2,1)}) %all-gather.14.cloned.1.call-update) | async-done | bytes 4194320 | tf_op jit(solution)/shard_map/all_gather | solution.py:97
  360.3 4.8 %copy.58 = bf16[2048,1024]{1,0:T(8,128)(2,1)} copy(bf16[2048,1024]{1,0:T(8,128)(2,1)} %all-gather.12.cloned.1.call-done) | data formatting | bytes 8388608
  365.1 2.0 copy.59
  (52 shorter events, 2.7 us)
Async XLA Ops:
  7.2 29.0 %copy-start = (bf16[512,1024]{1,0:T(8,128)(2,1)S(1)}, bf16[512,1024]{1,0:T(8,128)(2,1)}, u32[]{:S(2)}) copy-start(bf16[512,1024]{1,0:T(8,128)(2,1)} %param.16) | copy-start | bytes 3145732
  7.2 1.5 copy-start.3
  7.2 15.7 %all-gather.8.cloned.1.call-start = ((), (), s32[]{:S(2)}) async-start(), calls=%async_computation.2 | async-start | bytes 3145728 | tf_op jit(solution)/shard_map/all_gather | solution.py:54
  7.9 28.3 %all-gather.6.cloned.1.call-start = ((), (), s32[]{:S(2)}) async-start(), calls=%async_computation.1 | async-start | bytes 3145728 | tf_op jit(solution)/shard_map/all_gather | solution.py:53
  8.7 123.3 %reduce-scatter.4.cloned.1.call-start = ((), (), s32[]{:S(2)}) async-start(), calls=%async_computation.6 | async-start | bytes 2228224 | tf_op jit(solution)/shard_map/reduce_scatter | solution.py:74
  9.0 1.2 copy-start.2
  10.5 0.7 copy-start.15
  11.4 0.9 copy-start.16
  22.9 1.6 copy-start.5
  24.5 2.8 copy-start.8
  31.4 8.9 %copy-start.7 = (bf16[2048,256]{1,0:T(8,128)(2,1)S(1)}, bf16[2048,256]{1,0:T(8,128)(2,1)}, u32[]{:S(2)}) copy-start(bf16[2048,256]{1,0:T(8,128)(2,1)} %param.22) | copy-start | bytes 3145732
  49.1 82.9 %copy-start.11 = (f32[16,1024]{1,0:T(8,128)S(1)}, f32[16,1024]{1,0:T(8,128)}, u32[]{:S(2)}) copy-start(f32[16,1024]{1,0:T(8,128)} %param.29) | copy-start | bytes 196612
  49.1 82.9 %copy-start.12 = (f32[16,1024]{1,0:T(8,128)S(1)}, f32[16,1024]{1,0:T(8,128)}, u32[]{:S(2)}) copy-start(f32[16,1024]{1,0:T(8,128)} %param.27) | copy-start | bytes 196612
  49.1 82.9 %copy-start.13 = (f32[16,1024]{1,0:T(8,128)S(1)}, f32[16,1024]{1,0:T(8,128)}, u32[]{:S(2)}) copy-start(f32[16,1024]{1,0:T(8,128)} %param.28) | copy-start | bytes 196612
  49.1 82.9 %copy-start.14 = (f32[16,1024]{1,0:T(8,128)S(1)}, f32[16,1024]{1,0:T(8,128)}, u32[]{:S(2)}) copy-start(f32[16,1024]{1,0:T(8,128)} %param.26) | copy-start | bytes 196612
  49.2 143.0 %copy-start.9 = (f32[128,1024]{1,0:T(8,128)S(1)}, f32[128,1024]{1,0:T(8,128)}, u32[]{:S(2)}) copy-start(f32[128,1024]{1,0:T(8,128)} %param.24) | copy-start | bytes 1572868
  49.2 145.9 %copy-start.10 = (f32[1024,128]{1,0:T(8,128)S(1)}, f32[1024,128]{1,0:T(8,128)}, u32[]{:S(2)}) copy-start(f32[1024,128]{1,0:T(8,128)} %param.25) | copy-start | bytes 1572868
  49.2 143.0 %all-gather.10.cloned.1.call-start = ((), (), s32[]{:S(2)}) async-start(), calls=%async_computation.3 | async-start | bytes 2228224 | tf_op jit(solution)/shard_map/all_gather | solution.py:80
  133.7 136.1 %all-gather.12.cloned.1.call-start = ((), (), s32[]{:S(2)}) async-start(), calls=%async_computation.4 | async-start | bytes 4456448 | tf_op jit(solution)/shard_map/all_gather | solution.py:96
  192.2 2.9 copy-start.6
  195.0 165.3 %all-gather.14.cloned.1.call-start = ((), (), s32[]{:S(2)}) async-start(), calls=%async_computation.5 | async-start | bytes 4456448 | tf_op jit(solution)/shard_map/all_gather | solution.py:97
  360.3 4.8 %copy-start.4 = (bf16[1024,2048]{1,0:T(8,128)(2,1)S(1)}, bf16[1024,2048]{1,0:T(8,128)(2,1)}, u32[]{:S(2)}) copy-start(bf16[1024,2048]{1,0:T(8,128)(2,1)} %all-gather.14.cloned.1.call-done) | copy-start | bytes 12582916
  365.1 2.0 copy-start.1
Sparse Core Ops, SparseCore 0:
  9.5 13.2 all-gather.7
  24.4 11.7 all-gather.5
  49.3 82.6 reduce-scatter.3
  135.2 56.9 all-gather.9
  195.4 74.3 all-gather.11
  272.9 87.3 all-gather.13
where the time goes:
time: 374 us
  waiting for transfers between devices  319 us (85%)
  matrix products  23.3 us (6%)
  between operations  14.3 us (4%)
  local copies, waits for them, and re-layouts  13.8 us (4%)
    all_gather x1, waiting for transfers between devices, local(): lax.all_gather(output_master.astype(jnp.bfloat16), 'fs', axis=1, tiled=True)  90.5 us
    reduce_scatter x1, waiting for transfers between devices, local(): lax.psum_scatter(partial_value, 'fs', scatter_dimension=0, tiled=True)  82.7 us
    all_gather x1, waiting for transfers between devices, local(): lax.all_gather(value_master.astype(jnp.bfloat16), 'fs', axis=0, tiled=True)  70.7 us
    all_gather x1, waiting for transfers between devices, local(): full_direction = lax.all_gather(direction, 'fs', axis=0, tiled=True)  58.5 us
    unnamed x39, local copies, waits for them, and re-layouts  11.6 us
    dot_general x2, matrix products, contract_rows(): lax.dot_general(left, right, (((0,), (0,)), ((), ())), precision=lax.Prec...  10.9 us
    all_gather x1, waiting for transfers between devices, local(): lax.all_gather(output_cotangent, 'tp', axis=1, tiled=True)  10.5 us
  transfers between devices with their start and end apart: 6, of which 6 were waited for; matrix products, arithmetic and copies ran while one was open for 4% of the time, Pallas kernels for 0%

commit v1 on v0

--- a/solution.py
+++ b/solution.py
@@ -77,7 +77,9 @@
     moment_new = 0.8 * moments + 0.2 * own_rows
     second_new = 0.95 * seconds + 0.05 * own_rows * own_rows
     direction = moment_new / (jnp.sqrt(second_new) + 1e-08)
-    full_direction = lax.all_gather(direction, "fs", axis=0, tiled=True)
+    full_direction = jnp.concatenate(
+        lax.all_to_all(jnp.stack([direction] * lax.axis_size("fs")), "fs", 0, 0), axis=0
+    )
     step_value = jnp.dot(
         value_rows,
         full_direction[:, :head_cols],

time: 374 us -> 358 us (0.957)
  waiting for transfers between devices: 319 us -> 298 us
  starting transfers between devices: 0.24 us -> 4.05 us
    all_gather x1 -> x0, waiting for transfers between devices: 58.5 us -> none  [local(): full_direction = lax.all_gather(direction, 'fs', axis=0, tiled=True)]
    all_to_all x0 -> x1, waiting for transfers between devices: none -> 35.2 us  [local(): lax.all_to_all(jnp.stack([direction] * lax.axis_size('fs')), 'fs', 0, 0)]
    all_to_all x0 -> x1, starting transfers between devices: none -> 3.85 us  [local(): lax.all_to_all(jnp.stack([direction] * lax.axis_size('fs')), 'fs', 0, 0)]
    unnamed x39 -> x37, local copies, waits for them, and re-layouts: 11.6 us -> 11.6 us
where the time goes in v1:
time: 358 us; the launch traced here: 357 us
  waiting for transfers between devices  298 us (83%)
  matrix products  22.8 us (6%)
  local copies, waits for them, and re-layouts  15.3 us (4%)
  between operations  14 us (4%)
  starting transfers between devices  4.05 us (1%)
    all_gather x1, waiting for transfers between devices, local(): lax.all_gather(output_master.astype(jnp.bfloat16), 'fs', axis=1, tiled=True)  90.5 us
    reduce_scatter x1, waiting for transfers between devices, local(): lax.psum_scatter(partial_value, 'fs', scatter_dimension=0, tiled=True)  82.9 us
    all_gather x1, waiting for transfers between devices, local(): lax.all_gather(value_master.astype(jnp.bfloat16), 'fs', axis=0, tiled=True)  73.1 us
    all_to_all x1, waiting for transfers between devices, local(): lax.all_to_all(jnp.stack([direction] * lax.axis_size('fs')), 'fs', 0, 0)  35.2 us
    unnamed x37, local copies, waits for them, and re-layouts  11.6 us
    dot_general x2, matrix products, contract_rows(): lax.dot_general(left, right, (((0,), (0,)), ((), ())), precision=lax.Prec...  10.9 us
    all_gather x1, waiting for transfers between devices, local(): lax.all_gather(output_cotangent, 'tp', axis=1, tiled=True)  10.5 us
  transfers between devices with their start and end apart: 6, of which 6 were waited for; matrix products, arithmetic and copies ran while one was open for 4% of the time, Pallas kernels for 0%

profile of v1, /device:TPU:0, one launch (start us, length us, event | category | flops | bytes accessed | tf_op | source)
XLA Modules:
  0.0 357.1 jit_solution(2699826985882291915)
XLA Ops:
  7.2 0.7 all-gather.7.cloned.1.call-update
  8.0 0.7 all-gather.5.cloned.1.call-update
  9.5 0.7 copy-done.2
  12.4 10.5 %all-gather.7.cloned.1.call-done = bf16[512,2048]{1,0:T(8,128)(2,1)} async-done(((bf16[512,1024]{1,0:T(8,128)(2,1)}), bf16[512,2048]{1,0:T(8,128)(2,1)}) %all-gather.7.cloned.1.call-update) | async-done | bytes 2097168 | tf_op jit(solution)/shard_map/all_gather | solution.py:54
  23.5 1.0 copy-done.5
  24.5 2.8 fusion.18
  27.3 4.0 %fusion.13 = f32[256,1024]{0,1:T(8,128)S(1)} fusion(bf16[2048,256]{1,0:T(8,128)(2,1)S(1)} %copy-done.7, f32[1024,2048]{1,0:T(8,128)S(1)} %fusion.18), kind=kOutput, calls=%fused_computation.18 | convolution fusion | flops 6444548096 | bytes 10485760 | tf_op jit(solution)/shard_map/dot_general | solution.py:10
  31.4 4.8 %all-gather.5.cloned.1.call-done = bf16[512,2048]{1,0:T(8,128)(2,1)} async-done(((bf16[512,1024]{1,0:T(8,128)(2,1)}), bf16[512,2048]{1,0:T(8,128)(2,1)}) %all-gather.5.cloned.1.call-update) | async-done | bytes 2097168 | tf_op jit(solution)/shard_map/all_gather | solution.py:53
  36.2 4.0 %fusion.38 = f32[2048,1024]{1,0:T(8,128)S(1)} fusion(bf16[512,2048]{1,0:T(8,128)(2,1)} %all-gather.5.cloned.1.call-done, bf16[512,1024]{1,0:T(8,128)(2,1)S(1)} %copy-done), kind=kOutput, calls=%fused_computation.47 | convolution fusion | flops 2147483648 | bytes 11534336 | tf_op jit(solution)/shard_map/dot_general | solution.py:17
  40.2 6.9 %fusion.10 = f32[256,1024]{0,1:T(8,128)S(1)} fusion(bf16[2048,256]{1,0:T(8,128)(2,1)S(1)} %copy-done.6, f32[2048,1024]{1,0:T(8,128)S(1)} %fusion.38), kind=kOutput, calls=%fused_computation.17 | convolution fusion | flops 6444548096 | bytes 10485760 | tf_op jit(solution)/shard_map/dot_general | solution.py:10
  47.3 1.8 copy.50
  49.2 82.9 %reduce-scatter.4.cloned.1.call-done = f32[16,2048]{1,0:T(8,128)} async-done(((f32[256,2048]{1,0:T(8,128)}), f32[16,2048]{1,0:T(8,128)}) %reduce-scatter.4.cloned.1.call-update) | async-done | bytes 131088 | tf_op jit(solution)/shard_map/reduce_scatter | solution.py:74
  132.1 1.0 add_divide_fusion
  133.1 1.6 stack.2
  134.7 3.9 %all-to-all-start = ((f32[16,16,2048]{2,1,0:T(8,128)}), f32[16,16,2048]{2,1,0:T(8,128)S(1)}, u32[]{:S(2)}, u32[]{:S(2)}) async-start(f32[16,16,2048]{2,1,0:T(8,128)} %stack.2), calls=%async_computation | async-start | bytes 4194304 | tf_op jit(solution)/shard_map/all_to_all | solution.py:81
  138.6 35.2 %all-to-all-done = f32[16,16,2048]{2,1,0:T(8,128)S(1)} async-done(((f32[16,16,2048]{2,1,0:T(8,128)}), f32[16,16,2048]{2,1,0:T(8,128)S(1)}, u32[]{:S(2)}, u32[]{:S(2)}) %all-to-all-start) | async-done | bytes 2097184 | tf_op jit(solution)/shard_map/all_to_all | solution.py:81
  173.8 2.2 fusion.36
  176.1 2.7 fusion.37
  178.9 0.7 fusion.35
  179.5 0.7 fusion.34
  180.2 73.1 %all-gather.9.cloned.1.call-done = bf16[2048,1024]{1,0:T(8,128)(2,1)} async-done(((bf16[128,1024]{1,0:T(8,128)(2,1)}), bf16[2048,1024]{1,0:T(8,128)(2,1)}) %all-gather.9.cloned.1.call-update) | async-done | bytes 4194320 | tf_op jit(solution)/shard_map/all_gather | solution.py:98
  253.3 90.5 %all-gather.11.cloned.1.call-done = bf16[1024,2048]{1,0:T(8,128)(2,1)} async-done(((bf16[1024,128]{1,0:T(8,128)(2,1)}), bf16[1024,2048]{1,0:T(8,128)(2,1)}) %all-gather.11.cloned.1.call-update) | async-done | bytes 4194320 | tf_op jit(solution)/shard_map/all_gather | solution.py:99
  343.7 4.8 %copy.59 = bf16[2048,1024]{1,0:T(8,128)(2,1)} copy(bf16[2048,1024]{1,0:T(8,128)(2,1)} %all-gather.9.cloned.1.call-done) | data formatting | bytes 8388608
  348.6 2.0 copy.60
  (50 shorter events, 3.8 us)
Async XLA Ops:
  7.2 29.0 %copy-start = (bf16[512,1024]{1,0:T(8,128)(2,1)S(1)}, bf16[512,1024]{1,0:T(8,128)(2,1)}, u32[]{:S(2)}) copy-start(bf16[512,1024]{1,0:T(8,128)(2,1)} %param.16) | copy-start | bytes 3145732
  7.2 1.5 copy-start.3
  7.2 15.7 %all-gather.7.cloned.1.call-start = ((), (), s32[]{:S(2)}) async-start(), calls=%async_computation.3 | async-start | bytes 3145728 | tf_op jit(solution)/shard_map/all_gather | solution.py:54
  7.9 28.3 %all-gather.5.cloned.1.call-start = ((), (), s32[]{:S(2)}) async-start(), calls=%async_computation.2 | async-start | bytes 3145728 | tf_op jit(solution)/shard_map/all_gather | solution.py:53
  8.7 123.4 %reduce-scatter.4.cloned.1.call-start = ((), (), s32[]{:S(2)}) async-start(), calls=%async_computation.6 | async-start | bytes 2228224 | tf_op jit(solution)/shard_map/reduce_scatter | solution.py:74
  9.0 1.2 copy-start.2
  10.5 0.7 copy-start.14
  11.4 0.9 copy-start.15
  22.9 1.6 copy-start.5
  24.5 2.8 copy-start.7
  31.4 8.9 %copy-start.6 = (bf16[2048,256]{1,0:T(8,128)(2,1)S(1)}, bf16[2048,256]{1,0:T(8,128)(2,1)}, u32[]{:S(2)}) copy-start(bf16[2048,256]{1,0:T(8,128)(2,1)} %param.22) | copy-start | bytes 3145732
  49.1 83.0 %copy-start.10 = (f32[16,1024]{1,0:T(8,128)S(1)}, f32[16,1024]{1,0:T(8,128)}, u32[]{:S(2)}) copy-start(f32[16,1024]{1,0:T(8,128)} %param.29) | copy-start | bytes 196612
  49.1 83.0 %copy-start.11 = (f32[16,1024]{1,0:T(8,128)S(1)}, f32[16,1024]{1,0:T(8,128)}, u32[]{:S(2)}) copy-start(f32[16,1024]{1,0:T(8,128)} %param.27) | copy-start | bytes 196612
  49.1 83.0 %copy-start.12 = (f32[16,1024]{1,0:T(8,128)S(1)}, f32[16,1024]{1,0:T(8,128)}, u32[]{:S(2)}) copy-start(f32[16,1024]{1,0:T(8,128)} %param.28) | copy-start | bytes 196612
  49.1 83.0 %copy-start.13 = (f32[16,1024]{1,0:T(8,128)S(1)}, f32[16,1024]{1,0:T(8,128)}, u32[]{:S(2)}) copy-start(f32[16,1024]{1,0:T(8,128)} %param.26) | copy-start | bytes 196612
  134.7 39.1 %copy-start.8 = (f32[128,1024]{1,0:T(8,128)S(1)}, f32[128,1024]{1,0:T(8,128)}, u32[]{:S(2)}) copy-start(f32[128,1024]{1,0:T(8,128)} %param.24) | copy-start | bytes 1572868
  134.7 39.1 %all-to-all-start = ((f32[16,16,2048]{2,1,0:T(8,128)}), f32[16,16,2048]{2,1,0:T(8,128)S(1)}, u32[]{:S(2)}, u32[]{:S(2)}) async-start(f32[16,16,2048]{2,1,0:T(8,128)} %stack.2), calls=%async_computation | async-start | bytes 4194304 | tf_op jit(solution)/shard_map/all_to_all | solution.py:81
  138.5 37.5 %copy-start.9 = (f32[1024,128]{1,0:T(8,128)S(1)}, f32[1024,128]{1,0:T(8,128)}, u32[]{:S(2)}) copy-start(f32[1024,128]{1,0:T(8,128)} %param.25) | copy-start | bytes 1572868
  138.6 114.7 %all-gather.9.cloned.1.call-start = ((), (), s32[]{:S(2)}) async-start(), calls=%async_computation.4 | async-start | bytes 4456448 | tf_op jit(solution)/shard_map/all_gather | solution.py:98
  176.0 167.7 %all-gather.11.cloned.1.call-start = ((), (), s32[]{:S(2)}) async-start(), calls=%async_computation.5 | async-start | bytes 4456448 | tf_op jit(solution)/shard_map/all_gather | solution.py:99
  343.7 4.8 %copy-start.4 = (bf16[1024,2048]{1,0:T(8,128)(2,1)S(1)}, bf16[1024,2048]{1,0:T(8,128)(2,1)}, u32[]{:S(2)}) copy-start(bf16[1024,2048]{1,0:T(8,128)(2,1)} %all-gather.11.cloned.1.call-done) | copy-start | bytes 12582916
  348.6 2.0 copy-start.1
Sparse Core Ops, SparseCore 0:
  9.5 13.2 all-gather.6
  24.4 11.7 all-gather.4
  49.3 82.7 reduce-scatter.3
  176.2 77.0 all-gather.8
  256.4 87.3 all-gather.10
